TPU v7x, 32 devices: a whole 2x2x4 slice. The times are simulated.
32 devices in a mesh: rep: 2 (over x), fs: 8 (over z, y), tp: 2 (over core).
Axes of the slice: x: 2, y: 2, z: 4, core: 2. Of those that a mesh axis runs over, the one named last changes fastest.
Arguments:
- pre_gate: bfloat16 [12288, 4096], P(('rep', 'fs'), 'tp'), may hold values from -6 to 6
- pre_linear: bfloat16 [12288, 4096], P(('rep', 'fs'), 'tp'), may hold values from -6 to 6
- taps_gate: float32 [3, 4096], P(None, 'tp'), may hold values from -3.5 to 3.5
- taps_linear: float32 [3, 4096], P(None, 'tp'), may hold values from -3.5 to 3.5
- bias_gate: float32 [4096], P('tp'), may hold values from -3 to 3
- bias_linear: float32 [4096], P('tp'), may hold values from -3 to 3
- down_weight: bfloat16 [4096, 2048], P('tp', 'fs'), may hold values from -0.09375 to 0.09375
- out_grad: bfloat16 [12288, 2048], P(('rep', 'fs')), may hold values from -8 to 8
Outputs:
- grad_gate: bfloat16 [12288, 4096], P(('rep', 'fs'), 'tp')
- grad_linear: bfloat16 [12288, 4096], P(('rep', 'fs'), 'tp')
- grad_taps_gate: float32 [3, 4096], P(None, 'tp')
- grad_taps_linear: float32 [3, 4096], P(None, 'tp')
- grad_bias_gate: float32 [4096], P('tp')
- grad_bias_linear: float32 [4096], P('tp')
- grad_down: float32 [4096, 2048], P('tp', 'fs')
- row_norms: float32 [4096], P('tp')
All inputs are finite; a program needn't handle non-finite values.
Results may differ from a plain program's by a relative error of at most 0.0031.
Values may be sent and summed in bfloat16 or wider, within the bound.
A program may use at most 128 MiB of HBM per device.

v0:
```python
import jax
import jax.numpy as jnp
from jax import lax
from jax.sharding import PartitionSpec as P


def convolve(values, taps, bias):
    length = values.shape[0]
    padded = jnp.pad(values, ((2, 0), (0, 0)))
    return (
        taps[0] * padded[0:length]
        + taps[1] * padded[1 : length + 1]
        + taps[2] * padded[2 : length + 2]
        + bias
    )


def convolve_back(grads, taps):
    length = grads.shape[0]
    padded = jnp.pad(grads, ((0, 2), (0, 0)))
    return (
        taps[0] * padded[2 : length + 2]
        + taps[1] * padded[1 : length + 1]
        + taps[2] * padded[0:length]
    )


def tap_grads(grads, values):
    length = values.shape[0]
    padded = jnp.pad(values, ((2, 0), (0, 0)))
    return jnp.stack([jnp.sum(grads * padded[j : j + length], axis=0) for j in range(3)])


def local(
    pre_gate, pre_linear, taps_gate, taps_linear, bias_gate, bias_linear, down_weight, out_grad
):
    gate_in = pre_gate.astype(jnp.float32)
    linear_in = pre_linear.astype(jnp.float32)
    gate_pre = convolve(gate_in, taps_gate, bias_gate)
    linear_pre = convolve(linear_in, taps_linear, bias_linear)
    sigma = jax.nn.sigmoid(gate_pre)
    silu_val = gate_pre * sigma
    hidden = (silu_val * linear_pre).astype(jnp.bfloat16)
    columns = out_grad
    grad_hidden = lax.dot_general(
        columns,
        lax.all_gather(down_weight, "fs", axis=1, tiled=True),
        (((1,), (1,)), ((), ())),
        preferred_element_type=jnp.float32,
    )
    grad_gate_pre = grad_hidden * linear_pre * sigma * (1.0 + gate_pre * (1.0 - sigma))
    grad_linear_pre = grad_hidden * silu_val
    grad_gate = convolve_back(grad_gate_pre, taps_gate).astype(jnp.bfloat16)
    grad_linear = convolve_back(grad_linear_pre, taps_linear).astype(jnp.bfloat16)
    conv_parts = (
        tap_grads(grad_gate_pre, gate_in),
        tap_grads(grad_linear_pre, linear_in),
        jnp.sum(grad_gate_pre, axis=0),
        jnp.sum(grad_linear_pre, axis=0),
    )
    grad_taps_gate, grad_taps_linear, grad_bias_gate, grad_bias_linear = lax.psum(
        (conv_parts[0], conv_parts[1], conv_parts[2], conv_parts[3]), ("rep", "fs")
    )
    columns = out_grad
    partial_grad = lax.psum_scatter(
        lax.dot_general(
            columns, hidden, (((0,), (0,)), ((), ())), preferred_element_type=jnp.float32
        ),
        "fs",
        scatter_dimension=0,
        tiled=True,
    )
    summed = lax.psum(partial_grad, "rep")
    grad_down = summed.T
    row_norms = lax.psum(jnp.sum(grad_down * grad_down, axis=1), "fs")
    return (
        grad_gate,
        grad_linear,
        grad_taps_gate,
        grad_taps_linear,
        grad_bias_gate,
        grad_bias_linear,
        grad_down,
        row_norms,
    )


def solution(mesh):
    in_specs = (
        P(("rep", "fs"), "tp"),
        P(("rep", "fs"), "tp"),
        P(None, "tp"),
        P(None, "tp"),
        P("tp"),
        P("tp"),
        P("tp", "fs"),
        P(("rep", "fs"), None),
    )
    out_specs = (
        P(("rep", "fs"), "tp"),
        P(("rep", "fs"), "tp"),
        P(None, "tp"),
        P(None, "tp"),
        P("tp"),
        P("tp"),
        P("tp", "fs"),
        P("tp"),
    )
    return jax.shard_map(local, mesh=mesh, in_specs=in_specs, out_specs=out_specs, check_vma=False)
```

profile of v0, /device:TPU:0, one launch (start us, length us, event | category | flops | bytes accessed | tf_op | source)
XLA Modules:
  0.0 668.1 jit_solution(7865275278848254621)
XLA Ops:
  7.2 0.0 copy-start
  7.2 0.0 all-gather.2.cloned.1.call-start
  7.2 0.7 all-gather.2.cloned.1.call-update
  7.9 0.0 reduce-scatter.2.cloned.1.call-start
  8.0 0.0 copy-start.3
  8.0 5.6 convert_element_type.24
  13.5 0.0 copy-done.3
  13.5 0.0 copy-start.4
  13.5 0.0 copy-start.5
  13.5 0.0 copy-start.7
  13.5 3.4 convert_element_type.23
  17.0 0.0 copy-done.4
  17.0 0.0 copy-done.5
  17.0 120.7 %all-gather.2.cloned.1.call-done = bf16[2048,2048]{1,0:T(8,128)(2,1)} async-done(((bf16[2048,256]{1,0:T(8,128)(2,1)}), bf16[2048,2048]{1,0:T(8,128)(2,1)}) %all-gather.2.cloned.1.call-update) | async-done | bytes 8388624 | tf_op jit(solution)/shard_map/all_gather | solution.py:47
  137.7 0.0 copy-done
  137.7 0.0 copy-done.7
  137.7 0.0 copy-start.1
  137.7 0.0 copy-start.2
  137.7 0.0 copy-start.6
  137.8 25.9 %fusion.4 = (f32[2048]{0:T(1024)}, f32[2048]{0:T(1024)S(1)}, f32[2048]{0:T(1024)S(1)}, f32[2048]{0:T(1024)S(1)}, f32[768,2048]{1,0:T(8,128)}, /*index=5*/f32[768,2048]{1,0:T(8,128)}, f32[768,2048]{1,0:T(8,128)}) fusion(bf16[768,2048]{1,0:T(8,128)(2,1)} %param.9, f32[768,2048]{1,0:T(8,128)} %convert_element_type.23, f32[2048]{0:T(1024)S(1)} %copy-done.7, ...), kind=kOutput, calls=%fused_computation.24 | convolution fusion | flops 6472327168 | bytes 46202880 | tf_op jit(solution)/shard_map/dot_general | solution.py:45
  163.7 0.0 copy-done.1
  163.7 0.0 copy-done.2
  163.7 0.0 copy-done.6
  163.7 19.0 %fusion.5 = (f32[2048]{0:T(1024)}, f32[2048]{0:T(1024)S(1)}, f32[2048]{0:T(1024)S(1)}, f32[2048]{0:T(1024)S(1)}, f32[768,2048]{1,0:T(8,128)}, /*index=5*/f32[768,2048]{1,0:T(8,128)}, bf16[768,2048]{1,0:T(8,128)(2,1)}) fusion(bf16[768,2048]{1,0:T(8,128)(2,1)} %param.8, f32[768,2048]{1,0:T(8,128)S(1)} %copy-done.1, f32[768,2048]{1,0:T(8,128)} %get-tuple-element.25, ...), kind=kLoop, calls=%fused_computation.25 | loop fusion | flops 45604864 | bytes 50397184 | tf_op jit(solution)/shard_map/reduce_sum | solution.py:58
  182.7 15.2 %convolution_bitcast_fusion = f32[2048,2048]{0,1:T(8,128)} fusion(bf16[768,2048]{1,0:T(8,128)(2,1)S(1)} %copy-done, f32[768,2048]{1,0:T(8,128)} %get-tuple-element.27, f32[768,2048]{1,0:T(8,128)} %get-tuple-element.25), kind=kOutput, calls=%fused_computation | convolution fusion | flops 6451888128 | bytes 32505856 | tf_op jit(solution)/shard_map/dot_general | solution.py:66
  197.8 0.0 reduce-scatter.2.cloned.1.call-update
  197.9 0.0 all-reduce.8.cloned.1.call-start
  197.9 278.5 %reduce-scatter.2.cloned.1.call-done = f32[256,2048]{0,1:T(8,128)} async-done(((f32[2048,2048]{0,1:T(8,128)}), f32[256,2048]{0,1:T(8,128)}) %reduce-scatter.2.cloned.1.call-update) | async-done | bytes 2097168 | tf_op jit(solution)/shard_map/reduce_scatter | solution.py:65
  476.4 0.0 all-reduce.8.cloned.1.call-update
  476.5 0.0 all-reduce.10.cloned.1.call-start
  476.5 0.7 pad_maximum_fusion
  477.2 9.6 %add_convert_fusion.1 = bf16[768,2048]{1,0:T(8,128)(2,1)} fusion(f32[768,2048]{1,0:T(8,128)} %get-tuple-element.26, f32[2048]{0:T(1024)S(1)} %bitcast.28, f32[2048]{0:T(1024)S(1)} %bitcast.30, f32[2048]{0:T(1024)S(1)} %bitcast.26), kind=kLoop, calls=%fused_computation.9 | loop fusion | flops 9437184 | bytes 9461760 | tf_op jit(solution)/shard_map/convert_element_type | solution.py:53
  486.8 0.0 all-reduce.10.cloned.1.call-update
  486.8 54.0 %all-reduce.8.cloned.1.call-done = f32[2048,256]{1,0:T(8,128)} async-done(((f32[2048,256]{1,0:T(8,128)}), f32[2048,256]{1,0:T(8,128)}) %all-reduce.8.cloned.1.call-update) | async-done | bytes 2097168 | tf_op jit(solution)/shard_map/psum | solution.py:73
  540.8 1.9 multiply_reduce_fusion.6
  542.8 22.3 %psum.47 = f32[2048]{0:T(1024)} all-reduce(f32[2048]{0:T(1024)S(1)} %multiply_reduce_fusion.6), channel_id=1, replica_groups=mesh['rep'=2,'fs'=8,'tp'=2] {'fs'}, use_global_device_ids=true, to_apply=%region_15.16 | all-reduce | flops 2048 | bytes 16384 | tf_op jit(solution)/shard_map/psum | solution.py:75
  565.1 88.1 %all-reduce.10.cloned.1.call-done = (f32[3,2048]{1,0:T(4,128)}, f32[3,2048]{1,0:T(4,128)}, f32[2048]{0:T(1024)}, f32[2048]{0:T(1024)}) async-done(((f32[3,2048]{1,0:T(4,128)}, f32[3,2048]{1,0:T(4,128)}, f32[2048]{0:T(1024)}, f32[2048]{0:T(1024)}), (f32[3,2048]{1,0:T(4,128)}, f32[3,2048]{1,0:T(4,128)}, f32[2048]{0:T(1024)}, f32[2048]{0:T(1024)})) %all-reduce.10.cloned.1.call-update) | async-done | bytes 65552 | tf_op jit(solution)/shard_map/psum | solution.py:61
  653.2 1.4 copy.21
  654.6 1.4 copy.22
  655.9 1.3 copy.23
  657.2 1.3 copy.24
  658.5 3.0 copy.25
  (2 shorter events, 0.0 us)
Async XLA Ops:
  7.2 130.6 %copy-start = (bf16[768,2048]{1,0:T(8,128)(2,1)S(1)}, bf16[768,2048]{1,0:T(8,128)(2,1)}, u32[]{:S(2)}) copy-start(bf16[768,2048]{1,0:T(8,128)(2,1)} %param.15) | copy-start | bytes 9437188
  7.2 130.5 %all-gather.2.cloned.1.call-start = ((), (), s32[]{:S(2)}) async-start(), calls=%async_computation.1 | async-start | bytes 9437184 | tf_op jit(solution)/shard_map/all_gather | solution.py:47
  7.9 468.5 %reduce-scatter.2.cloned.1.call-start = ((), (), s32[]{:S(2)}) async-start(), calls=%async_computation.2 | async-start | bytes 18874368 | tf_op jit(solution)/shard_map/reduce_scatter | solution.py:65
  8.0 5.6 copy-start.3
  13.5 3.4 copy-start.4
  13.5 3.5 copy-start.5
  13.5 124.2 %copy-start.7 = (f32[2048]{0:T(1024)S(1)}, f32[2048]{0:T(1024)}, u32[]{:S(2)}) copy-start(f32[2048]{0:T(1024)} %param.12) | copy-start | bytes 24580
  137.7 25.9 %copy-start.1 = (f32[768,2048]{1,0:T(8,128)S(1)}, f32[768,2048]{1,0:T(8,128)}, u32[]{:S(2)}) copy-start(f32[768,2048]{1,0:T(8,128)} %convert_element_type.24) | copy-start | bytes 18874372
  137.7 25.9 %copy-start.2 = (f32[768,2048]{1,0:T(8,128)S(1)}, f32[768,2048]{1,0:T(8,128)}, u32[]{:S(2)}) copy-start(f32[768,2048]{1,0:T(8,128)} %convert_element_type.23) | copy-start | bytes 18874372
  137.7 25.9 %copy-start.6 = (f32[2048]{0:T(1024)S(1)}, f32[2048]{0:T(1024)}, u32[]{:S(2)}) copy-start(f32[2048]{0:T(1024)} %param.13) | copy-start | bytes 24580
  197.9 343.0 %all-reduce.8.cloned.1.call-start = ((), (), s32[]{:S(2)}) async-start(), calls=%async_computation.3 | async-start | bytes 4194304 | tf_op jit(solution)/shard_map/psum | solution.py:73
  476.5 176.7 %all-reduce.10.cloned.1.call-start = ((), (), s32[]{:S(2)}) async-start(), calls=%async_computation.4 | async-start | bytes 163840 | tf_op jit(solution)/shard_map/psum | solution.py:61
Sparse Core Ops, SparseCore 0:
  10.0 127.6 all-gather.1
  198.0 278.3 reduce-scatter.1
  478.7 62.0 all-reduce.7
  547.2 105.9 all-reduce.9
where the time goes:
time: 669 us; the launch traced here: 668 us
  waiting for transfers between devices  542 us (81%)
  matrix products  41.1 us (6%)
  other arithmetic  40.2 us (6%)
  blocking collectives  22.3 us (3%)
  between operations  13.8 us (2%)
  local copies, waits for them, and re-layouts  8.47 us (1%)
    reduce_scatter x1, waiting for transfers between devices, local(): lax.psum_scatter(lax.dot_general(columns, hidden, (((0,), (0,)), ((), ())...  279 us
    all_gather x1, waiting for transfers between devices, local(): lax.all_gather(down_weight, 'fs', axis=1, tiled=True)  121 us
    psum x1, waiting for transfers between devices, local(): lax.psum((conv_parts[0], conv_parts[1], conv_parts[2], conv_parts[3]), ('...  88.1 us
    psum x1, waiting for transfers between devices, local(): summed = lax.psum(partial_grad, 'rep')  54 us
    dot_general x1, matrix products, local(): lax.dot_general(columns, lax.all_gather(down_weight, 'fs', axis=1, tiled=...  25.9 us
    psum x1, blocking collectives, local(): row_norms = lax.psum(jnp.sum(grad_down * grad_down, axis=1), 'fs')  22.3 us
    reduce_sum x1, other arithmetic, local(): jnp.sum(grad_gate_pre, axis=0)  19 us
    dot_general x1, matrix products, local(): lax.dot_general(columns, hidden, (((0,), (0,)), ((), ())), preferred_elem...  15.2 us
  transfers between devices with their start and end apart: 4, of which 4 were waited for; matrix products, arithmetic and copies ran while one was open for 3% of the time, Pallas kernels for 0%

commit v1 on v0

v1 whole, which is shorter than its diff:
```python
import functools

import jax
import jax.numpy as jnp
from jax import lax
from jax.experimental import pallas as pl
from jax.experimental.pallas import tpu as pltpu
from jax.sharding import PartitionSpec as P

MESH = pl.DeviceIdType.MESH


def shift_down(values, steps):
    if steps == 0:
        return values
    rows = lax.broadcasted_iota(jnp.int32, values.shape, 0)
    return jnp.where(rows < steps, 0.0, pltpu.roll(values, steps, 0))


def shift_up(values, steps):
    length = values.shape[0]
    rows = lax.broadcasted_iota(jnp.int32, values.shape, 0)
    return jnp.where(rows >= length - steps, 0.0, pltpu.roll(values, length - steps, 0))


def conv_chunk(values, taps, bias):
    return (
        taps[0:1] * shift_down(values, 2)
        + taps[1:2] * shift_down(values, 1)
        + taps[2:3] * values
        + bias
    )


def conv_back_chunk(grads, taps):
    return taps[0:1] * shift_up(grads, 2) + taps[1:2] * shift_up(grads, 1) + taps[2:3] * grads


def kernel(
    fs, chunk,
    pg_ref, pl_ref, tg_ref, tl_ref, bg_ref, bl_ref, w_ref, og_ref,
    gg_ref, gl_ref, cp_ref, gd_ref, rn_ref,
    wbuf, sbuf, rbuf, xs, xr, cpbuf, cps, cpx, rnbuf,
    w_send, w_recv, f_send, f_recv, s_send, s_recv, x_send, x_recv,
    c_send, c_recv, cx_send, cx_recv, n_send, n_recv,
):
    me = lax.axis_index("fs")
    rep = lax.axis_index("rep")
    partner = 1 - rep
    tokens, ff = pg_ref.shape
    dc = w_ref.shape[1]
    chunks = ff // chunk
    half = ff // 2
    per = -(-(fs - 1) // chunks)

    def to(k):
        return lax.rem(me + k, fs)

    def source(k):
        return lax.rem(me + fs - k, fs)

    def rows_of(c):
        return pl.ds(pl.multiple_of(c * chunk, chunk), chunk)

    def w_copy(k):
        rows = pl.ds(pl.multiple_of(rep * half, half), half)
        return pltpu.make_async_remote_copy(
            src_ref=w_ref.at[rows], dst_ref=wbuf.at[me, rows],
            send_sem=w_send.at[k], recv_sem=w_recv.at[k],
            device_id={"fs": to(k)}, device_id_type=MESH)

    def f_copy(k):
        rows = pl.ds(pl.multiple_of(rep * half, half), half)
        return pltpu.make_async_remote_copy(
            src_ref=wbuf.at[source(k), rows], dst_ref=wbuf.at[source(k), rows],
            send_sem=f_send.at[k], recv_sem=f_recv.at[k],
            device_id={"rep": partner}, device_id_type=MESH)

    def s_copy(c, k):
        return pltpu.make_async_remote_copy(
            src_ref=sbuf.at[to(k), rows_of(c)], dst_ref=rbuf.at[k, rows_of(c)],
            send_sem=s_send.at[c, k], recv_sem=s_recv.at[c, k],
            device_id={"fs": to(k)}, device_id_type=MESH)

    def x_copy(c):
        return pltpu.make_async_remote_copy(
            src_ref=xs.at[rows_of(c)], dst_ref=xr.at[rows_of(c)],
            send_sem=x_send.at[c], recv_sem=x_recv.at[c],
            device_id={"rep": partner}, device_id_type=MESH)

    def c_copy(k):
        return pltpu.make_async_remote_copy(
            src_ref=cpbuf.at[me], dst_ref=cpbuf.at[me],
            send_sem=c_send.at[k], recv_sem=c_recv.at[k],
            device_id={"fs": to(k)}, device_id_type=MESH)

    def cx_copy():
        return pltpu.make_async_remote_copy(
            src_ref=cps, dst_ref=cpx, send_sem=cx_send, recv_sem=cx_recv,
            device_id={"rep": partner}, device_id_type=MESH)

    def n_copy(k):
        return pltpu.make_async_remote_copy(
            src_ref=rnbuf.at[me], dst_ref=rnbuf.at[me],
            send_sem=n_send.at[k], recv_sem=n_recv.at[k],
            device_id={"fs": to(k)}, device_id_type=MESH)

    barrier = pltpu.get_barrier_semaphore()

    @pl.loop(1, fs)
    def _(k):
        pl.semaphore_signal(barrier, inc=1, device_id={"fs": to(k)}, device_id_type=MESH)

    pl.semaphore_signal(barrier, inc=1, device_id={"rep": partner}, device_id_type=MESH)
    pl.semaphore_wait(barrier, fs)

    @pl.loop(1, fs)
    def _(k):
        w_copy(k).start()

    wbuf[me] = w_ref[...]

    @pl.loop(0, chunks)
    def _(c):
        cols = rows_of(c)
        gate_pre = conv_chunk(
            pg_ref[:, cols].astype(jnp.float32), tg_ref[:, cols], bg_ref[:, cols])
        linear_pre = conv_chunk(
            pl_ref[:, cols].astype(jnp.float32), tl_ref[:, cols], bl_ref[:, cols])
        hidden = (gate_pre * jax.nn.sigmoid(gate_pre) * linear_pre).astype(jnp.bfloat16)
        for j in range(fs):
            part = lax.dot_general(
                hidden, og_ref[:, j * dc:(j + 1) * dc], (((0,), (0,)), ((), ())),
                preferred_element_type=jnp.float32)
            sbuf[j, cols] = part.astype(jnp.bfloat16)

        @pl.loop(1, fs)
        def _(k):
            s_copy(c, k).start()

        for step in range(per):
            k = c * per + step + 1

            @pl.when(k < fs)
            def _():
                w_copy(k).wait_recv()
                f_copy(k).start()

    @pl.loop(1, fs)
    def _(k):
        f_copy(k).wait_recv()

    @pl.loop(0, chunks)
    def _(c):
        cols = rows_of(c)
        gate_in = pg_ref[:, cols].astype(jnp.float32)
        linear_in = pl_ref[:, cols].astype(jnp.float32)
        taps_gate, taps_linear = tg_ref[:, cols], tl_ref[:, cols]
        gate_pre = conv_chunk(gate_in, taps_gate, bg_ref[:, cols])
        linear_pre = conv_chunk(linear_in, taps_linear, bl_ref[:, cols])
        sigma = jax.nn.sigmoid(gate_pre)
        grad_hidden = jnp.zeros((tokens, chunk), jnp.float32)
        for j in range(fs):
            grad_hidden += lax.dot_general(
                og_ref[:, j * dc:(j + 1) * dc], wbuf[j, cols], (((1,), (1,)), ((), ())),
                preferred_element_type=jnp.float32)
        grad_gate_pre = grad_hidden * linear_pre * sigma * (1.0 + gate_pre * (1.0 - sigma))
        grad_linear_pre = grad_hidden * (gate_pre * sigma)
        gg_ref[:, cols] = conv_back_chunk(grad_gate_pre, taps_gate).astype(jnp.bfloat16)
        gl_ref[:, cols] = conv_back_chunk(grad_linear_pre, taps_linear).astype(jnp.bfloat16)
        for j in range(3):
            cpbuf[me, j:j + 1, cols] = jnp.sum(
                grad_gate_pre * shift_down(gate_in, 2 - j), axis=0, keepdims=True)
            cpbuf[me, j + 3:j + 4, cols] = jnp.sum(
                grad_linear_pre * shift_down(linear_in, 2 - j), axis=0, keepdims=True)
        cpbuf[me, 6:7, cols] = jnp.sum(grad_gate_pre, axis=0, keepdims=True)
        cpbuf[me, 7:8, cols] = jnp.sum(grad_linear_pre, axis=0, keepdims=True)

        @pl.when(c == chunks - 1)
        def _():
            @pl.loop(1, fs)
            def _(k):
                c_copy(k).start()

        total = sbuf[me, cols].astype(jnp.float32)
        for k in range(1, fs):
            s_copy(c, k).wait_recv()
            total += rbuf[k, cols].astype(jnp.float32)
        xs[cols] = total
        x_copy(c).start()

    @pl.loop(1, fs)
    def _(k):
        c_copy(k).wait_recv()

    sums = cpbuf[0]
    for j in range(1, fs):
        sums += cpbuf[j]
    cps[...] = sums
    cx_copy().start()

    @pl.loop(0, chunks)
    def _(c):
        rows = rows_of(c)
        x_copy(c).wait_recv()
        total = xs[rows] + xr[rows]
        gd_ref[rows] = total
        square = total * total
        while square.shape[1] % 256 == 0:
            middle = square.shape[1] // 2
            square = square[:, :middle] + square[:, middle:]
        rnbuf[me, 0:1, rows] = jnp.sum(square.T, axis=0, keepdims=True)

    @pl.loop(1, fs)
    def _(k):
        n_copy(k).start()

    cx_copy().wait_recv()
    cp_ref[...] = cps[...] + cpx[...]

    @pl.loop(1, fs)
    def _(k):
        n_copy(k).wait_recv()

    norms = rnbuf[0]
    for j in range(1, fs):
        norms += rnbuf[j]
    rn_ref[...] = norms

    cx_copy().wait_send()

    @pl.loop(1, fs)
    def _(k):
        w_copy(k).wait_send()
        f_copy(k).wait_send()
        c_copy(k).wait_send()
        n_copy(k).wait_send()

    @pl.loop(0, chunks)
    def _(c):
        x_copy(c).wait_send()

        @pl.loop(1, fs)
        def _(k):
            s_copy(c, k).wait_send()


def local(
    fs, pre_gate, pre_linear, taps_gate, taps_linear, bias_gate, bias_linear, down_weight, out_grad
):
    tokens, ff = pre_gate.shape
    dc = down_weight.shape[1]
    chunk = 256
    chunks = ff // chunk
    f32, bf16 = jnp.float32, jnp.bfloat16
    vmem = pl.BlockSpec(memory_space=pltpu.VMEM)
    dma = pltpu.SemaphoreType.DMA
    gg, gl, cp, gd, rn = pl.pallas_call(
        functools.partial(kernel, fs, chunk),
        out_shape=(
            jax.ShapeDtypeStruct((tokens, ff), bf16),
            jax.ShapeDtypeStruct((tokens, ff), bf16),
            jax.ShapeDtypeStruct((8, ff), f32),
            jax.ShapeDtypeStruct((ff, dc), f32),
            jax.ShapeDtypeStruct((1, ff), f32),
        ),
        in_specs=[vmem] * 8,
        out_specs=(vmem,) * 5,
        scratch_shapes=[
            pltpu.VMEM((fs, ff, dc), bf16),
            pltpu.VMEM((fs, ff, dc), bf16),
            pltpu.VMEM((fs, ff, dc), bf16),
            pltpu.VMEM((ff, dc), f32),
            pltpu.VMEM((ff, dc), f32),
            pltpu.VMEM((fs, 8, ff), f32),
            pltpu.VMEM((8, ff), f32),
            pltpu.VMEM((8, ff), f32),
            pltpu.VMEM((fs, 1, ff), f32),
            dma((fs,)), dma((fs,)), dma((fs,)), dma((fs,)),
            dma((chunks, fs)), dma((chunks, fs)), dma((chunks,)), dma((chunks,)),
            dma((fs,)), dma((fs,)), dma, dma, dma((fs,)), dma((fs,)),
        ],
        compiler_params=pltpu.CompilerParams(
            collective_id=0, has_side_effects=True, vmem_limit_bytes=67043328),
    )(pre_gate, pre_linear, taps_gate, taps_linear, bias_gate[None], bias_linear[None],
      down_weight, out_grad)
    return gg, gl, cp[0:3], cp[3:6], cp[6], cp[7], gd, rn[0]


def solution(mesh):
    in_specs = (
        P(("rep", "fs"), "tp"),
        P(("rep", "fs"), "tp"),
        P(None, "tp"),
        P(None, "tp"),
        P("tp"),
        P("tp"),
        P("tp", "fs"),
        P(("rep", "fs"), None),
    )
    out_specs = (
        P(("rep", "fs"), "tp"),
        P(("rep", "fs"), "tp"),
        P(None, "tp"),
        P(None, "tp"),
        P("tp"),
        P("tp"),
        P("tp", "fs"),
        P("tp"),
    )
    return jax.shard_map(
        functools.partial(local, mesh.shape["fs"]), mesh=mesh, in_specs=in_specs, out_specs=out_specs, check_vma=False)
```

time: 669 us -> 318 us (0.48)
  waiting for transfers between devices: 542 us -> 0 us
  Pallas kernels: 0 us -> 305 us
  matrix products: 41.1 us -> 0 us
  other arithmetic: 40.2 us -> 0 us
  blocking collectives: 22.3 us -> 0 us
  between operations: 13.8 us -> 0.65 us
    pallas_call x0 -> x1, Pallas kernels: none -> 305 us  [local(): pl.pallas_call(functools.partial(kernel, fs, chunk), out_shape=(jax.Shape...]
    reduce_scatter x1 -> x0, waiting for transfers between devices: 279 us -> none  [local(): lax.psum_scatter(lax.dot_general(columns, hidden, (((0,), (0,)), ((), ())...]
    psum x2 -> x0, waiting for transfers between devices: 142 us -> none  [the longest x1 88.1 us: local(): lax.psum((conv_parts[0], conv_parts[1], conv_parts[2], conv_parts[3]), ('...]
    all_gather x1 -> x0, waiting for transfers between devices: 121 us -> none  [local(): lax.all_gather(down_weight, 'fs', axis=1, tiled=True)]
    dot_general x2 -> x0, matrix products: 41.1 us -> none  [the longest x1 25.9 us: local(): lax.dot_general(columns, lax.all_gather(down_weight, 'fs', axis=1, tiled=...]
    psum x1 -> x0, blocking collectives: 22.3 us -> none  [local(): row_norms = lax.psum(jnp.sum(grad_down * grad_down, axis=1), 'fs')]
    reduce_sum x2 -> x0, other arithmetic: 20.9 us -> none  [the longest x1 19 us: local(): jnp.sum(grad_gate_pre, axis=0)]
    convert_element_type x3 -> x0, other arithmetic: 18.6 us -> none  [the longest x1 9.61 us: local(): grad_gate = convolve_back(grad_gate_pre, taps_gate).astype(jnp.bfloat16)]
  transfers between devices with their start and end apart: 4 -> 0, of which waited for: 4 -> 0; matrix products, arithmetic and copies ran while one was open for 3% -> 0% of each run, Pallas kernels for 0% -> 0%
where the time goes in v1:
time: 318 us; the launch traced here: 317 us
  Pallas kernels  305 us (96%)
  local copies, waits for them, and re-layouts  11.8 us (4%)
    pallas_call x1, Pallas kernels, local(): pl.pallas_call(functools.partial(kernel, fs, chunk), out_shape=(jax.Shape...  305 us
    unnamed x10, local copies, waits for them, and re-layouts  8.77 us

profile of v1, /device:TPU:0, one launch (start us, length us, event | category | flops | bytes accessed | tf_op | source)
XLA Modules:
  0.0 317.4 jit_solution(804761919366987298)
XLA Ops:
  0.6 304.9 %shard_map.143 = (bf16[768,2048]{1,0:T(8,128)(2,1)}, bf16[768,2048]{1,0:T(8,128)(2,1)}, f32[8,2048]{1,0:T(8,128)}, f32[2048,256]{1,0:T(8,128)}, f32[1,2048]{1,0:T(1,128)}) custom-call(bf16[768,2048]{1,0:T(8,128)(2,1)} %pg_ref.1, bf16[768,2048]{1,0:T(8,128)(2,1)} %pl_ref.1, f32[3,2048]{1,0:T(4,128)} %tg_ref.1, f32[3,2048]{1,0:T(4,128)} %tl_ref.1, ...), custom_call_target="tpu_custom_call" | custom-call | tf_op jit(solution)/shard_map/pallas_call | solution.py:258
  305.6 1.6 fusion.1
  307.1 1.5 fusion
  308.7 0.0 copy-start
  308.7 4.1 %copy.20 = bf16[768,2048]{1,0:T(8,128)(2,1)} copy(bf16[768,2048]{1,0:T(8,128)(2,1)} %get-tuple-element.30) | data formatting | bytes 6291456
  312.8 0.0 copy-done
  312.8 0.0 copy-start.1
  312.8 1.7 copy.21
  314.4 1.1 copy-done.1
  315.5 0.0 copy-start.2
  315.5 1.3 copy.22
  316.8 0.0 copy-done.2
  316.8 0.6 copy.23
Async XLA Ops:
  308.7 4.1 %copy-start = (bf16[768,2048]{1,0:T(8,128)(2,1)S(1)}, bf16[768,2048]{1,0:T(8,128)(2,1)}, u32[]{:S(2)}) copy-start(bf16[768,2048]{1,0:T(8,128)(2,1)} %get-tuple-element.31) | copy-start | bytes 9437188
  312.8 2.7 copy-start.1
  315.5 1.3 copy-start.2

commit v2 on v1

--- a/solution.py
+++ b/solution.py
@@ -40,47 +40,89 @@
     fs, chunk,
     pg_ref, pl_ref, tg_ref, tl_ref, bg_ref, bl_ref, w_ref, og_ref,
     gg_ref, gl_ref, cp_ref, gd_ref, rn_ref,
-    wbuf, sbuf, rbuf, xs, xr, cpbuf, cps, cpx, rnbuf,
-    w_send, w_recv, f_send, f_recv, s_send, s_recv, x_send, x_recv,
+    wbuf, sbuf, pbuf, rbuf, xs, xr, cpbuf, cps, cpx, rnbuf,
+    w_send, w_recv, y_send, y_recv, p_send, p_recv, f_send, f_recv, s_send, s_recv, x_send, x_recv,
     c_send, c_recv, cx_send, cx_recv, n_send, n_recv,
 ):
     me = lax.axis_index("fs")
     rep = lax.axis_index("rep")
     partner = 1 - rep
+    pairs = fs // 2
+    z = me // 2
+    par = me % 2
+    mate = me + 1 - 2 * par
     tokens, ff = pg_ref.shape
     dc = w_ref.shape[1]
     chunks = ff // chunk
     half = ff // 2
+    lag = chunks // 2
     per = -(-(fs - 1) // chunks)
 
     def to(k):
         return lax.rem(me + k, fs)
 
-    def source(k):
-        return lax.rem(me + fs - k, fs)
-
     def rows_of(c):
         return pl.ds(pl.multiple_of(c * chunk, chunk), chunk)
 
+    def shard(z_at, parity):
+        return z_at * 2 + parity
+
+    def z_to(k):
+        return lax.rem(z + k, pairs)
+
+    def z_from(k):
+        return lax.rem(z + pairs - k, pairs)
+
+    def my_half():
+        return pl.ds(pl.multiple_of(rep * half, half), half)
+
     def w_copy(k):
-        rows = pl.ds(pl.multiple_of(rep * half, half), half)
-        return pltpu.make_async_remote_copy(
-            src_ref=w_ref.at[rows], dst_ref=wbuf.at[me, rows],
+        return pltpu.make_async_remote_copy(
+            src_ref=w_ref.at[my_half()], dst_ref=wbuf.at[me, my_half()],
             send_sem=w_send.at[k], recv_sem=w_recv.at[k],
-            device_id={"fs": to(k)}, device_id_type=MESH)
-
-    def f_copy(k):
-        rows = pl.ds(pl.multiple_of(rep * half, half), half)
-        return pltpu.make_async_remote_copy(
-            src_ref=wbuf.at[source(k), rows], dst_ref=wbuf.at[source(k), rows],
-            send_sem=f_send.at[k], recv_sem=f_recv.at[k],
+            device_id={"fs": shard(z_to(k), par)}, device_id_type=MESH)
+
+    def y_first():
+        return pltpu.make_async_remote_copy(
+            src_ref=w_ref.at[my_half()], dst_ref=wbuf.at[me, my_half()],
+            send_sem=y_send.at[0], recv_sem=y_recv.at[0],
+            device_id={"fs": mate}, device_id_type=MESH)
+
+    def y_copy(k):
+        block = wbuf.at[shard(z_from(k), par), my_half()]
+        return pltpu.make_async_remote_copy(
+            src_ref=block, dst_ref=block,
+            send_sem=y_send.at[k], recv_sem=y_recv.at[k],
+            device_id={"fs": mate}, device_id_type=MESH)
+
+    def f_copy(item):
+        block = wbuf.at[shard(z_from(item % pairs), (par + item // pairs) % 2), my_half()]
+        return pltpu.make_async_remote_copy(
+            src_ref=block, dst_ref=block,
+            send_sem=f_send.at[item], recv_sem=f_recv.at[item],
             device_id={"rep": partner}, device_id_type=MESH)
 
+    def p_copy(c):
+        return pltpu.make_async_remote_copy(
+            src_ref=sbuf.at[1 - par, :, rows_of(c)], dst_ref=pbuf.at[:, rows_of(c)],
+            send_sem=p_send.at[c], recv_sem=p_recv.at[c],
+            device_id={"fs": mate}, device_id_type=MESH)
+
     def s_copy(c, k):
         return pltpu.make_async_remote_copy(
-            src_ref=sbuf.at[to(k), rows_of(c)], dst_ref=rbuf.at[k, rows_of(c)],
+            src_ref=sbuf.at[par, z_to(k), rows_of(c)], dst_ref=rbuf.at[k, rows_of(c)],
             send_sem=s_send.at[c, k], recv_sem=s_recv.at[c, k],
-            device_id={"fs": to(k)}, device_id_type=MESH)
+            device_id={"fs": shard(z_to(k), par)}, device_id_type=MESH)
+
+    def pair_sum(c):
+        p_copy(c).wait_recv()
+        for at in range(pairs):
+            both = sbuf[par, at, rows_of(c)].astype(jnp.float32) + pbuf[at, rows_of(c)].astype(jnp.float32)
+            sbuf[par, at, rows_of(c)] = both.astype(jnp.bfloat16)
+
+        @pl.loop(1, pairs)
+        def _(k):
+            s_copy(c, k).start()
 
     def x_copy(c):
         return pltpu.make_async_remote_copy(
@@ -114,7 +156,9 @@
     pl.semaphore_signal(barrier, inc=1, device_id={"rep": partner}, device_id_type=MESH)
     pl.semaphore_wait(barrier, fs)
 
-    @pl.loop(1, fs)
+    y_first().start()
+
+    @pl.loop(1, pairs)
     def _(k):
         w_copy(k).start()
 
@@ -132,18 +176,26 @@
             part = lax.dot_general(
                 hidden, og_ref[:, j * dc:(j + 1) * dc], (((0,), (0,)), ((), ())),
                 preferred_element_type=jnp.float32)
-            sbuf[j, cols] = part.astype(jnp.bfloat16)
-
-        @pl.loop(1, fs)
-        def _(k):
-            s_copy(c, k).start()
+            sbuf[j % 2, j // 2, cols] = part.astype(jnp.bfloat16)
+
+        p_copy(c).start()
+
+        @pl.when(c >= lag)
+        def _():
+            pair_sum(c - lag)
 
         for step in range(per):
             k = c * per + step + 1
 
-            @pl.when(k < fs)
+            @pl.when(k < pairs)
             def _():
                 w_copy(k).wait_recv()
+                y_copy(k).start()
+                f_copy(k).start()
+
+            @pl.when((k >= pairs) & (k < fs))
+            def _():
+                y_copy(k - pairs).wait_recv()
                 f_copy(k).start()
 
     @pl.loop(1, fs)
@@ -182,8 +234,12 @@
             def _(k):
                 c_copy(k).start()
 
-        total = sbuf[me, cols].astype(jnp.float32)
-        for k in range(1, fs):
+        @pl.when(c < lag)
+        def _():
+            pair_sum(chunks - lag + c)
+
+        total = sbuf[par, z, cols].astype(jnp.float32)
+        for k in range(1, pairs):
             s_copy(c, k).wait_recv()
             total += rbuf[k, cols].astype(jnp.float32)
         xs[cols] = total
@@ -228,10 +284,15 @@
     rn_ref[...] = norms
 
     cx_copy().wait_send()
-
-    @pl.loop(1, fs)
+    y_first().wait_send()
+
+    @pl.loop(1, pairs)
     def _(k):
         w_copy(k).wait_send()
+        y_copy(k).wait_send()
+
+    @pl.loop(1, fs)
+    def _(k):
         f_copy(k).wait_send()
         c_copy(k).wait_send()
         n_copy(k).wait_send()
@@ -239,8 +300,9 @@
     @pl.loop(0, chunks)
     def _(c):
         x_copy(c).wait_send()
-
-        @pl.loop(1, fs)
+        p_copy(c).wait_send()
+
+        @pl.loop(1, pairs)
         def _(k):
             s_copy(c, k).wait_send()
 
@@ -252,6 +314,7 @@
     dc = down_weight.shape[1]
     chunk = 256
     chunks = ff // chunk
+    pairs = fs // 2
     f32, bf16 = jnp.float32, jnp.bfloat16
     vmem = pl.BlockSpec(memory_space=pltpu.VMEM)
     dma = pltpu.SemaphoreType.DMA
@@ -268,16 +331,18 @@
         out_specs=(vmem,) * 5,
         scratch_shapes=[
             pltpu.VMEM((fs, ff, dc), bf16),
-            pltpu.VMEM((fs, ff, dc), bf16),
-            pltpu.VMEM((fs, ff, dc), bf16),
+            pltpu.VMEM((2, pairs, ff, dc), bf16),
+            pltpu.VMEM((pairs, ff, dc), bf16),
+            pltpu.VMEM((pairs, ff, dc), bf16),
             pltpu.VMEM((ff, dc), f32),
             pltpu.VMEM((ff, dc), f32),
             pltpu.VMEM((fs, 8, ff), f32),
             pltpu.VMEM((8, ff), f32),
             pltpu.VMEM((8, ff), f32),
             pltpu.VMEM((fs, 1, ff), f32),
-            dma((fs,)), dma((fs,)), dma((fs,)), dma((fs,)),
-            dma((chunks, fs)), dma((chunks, fs)), dma((chunks,)), dma((chunks,)),
+            dma((pairs,)), dma((pairs,)), dma((pairs,)), dma((pairs,)),
+            dma((chunks,)), dma((chunks,)), dma((fs,)), dma((fs,)),
+            dma((chunks, pairs)), dma((chunks, pairs)), dma((chunks,)), dma((chunks,)),
             dma((fs,)), dma((fs,)), dma, dma, dma((fs,)), dma((fs,)),
         ],
         compiler_params=pltpu.CompilerParams(

time: 318 us -> 200 us (0.63)
  Pallas kernels: 305 us -> 188 us
    pallas_call x1, Pallas kernels: 305 us -> 188 us  [local(): pl.pallas_call(functools.partial(kernel, fs, chunk), out_shape=(jax.Shape...]
where the time goes in v2:
time: 200 us
  Pallas kernels  188 us (94%)
  local copies, waits for them, and re-layouts  11.8 us (6%)
    pallas_call x1, Pallas kernels, local(): pl.pallas_call(functools.partial(kernel, fs, chunk), out_shape=(jax.Shape...  188 us
    unnamed x10, local copies, waits for them, and re-layouts  8.77 us

profile of v2, /device:TPU:0, one launch (start us, length us, event | category | flops | bytes accessed | tf_op | source)
XLA Modules:
  0.0 200.1 jit_solution(16658635276145665691)
XLA Ops:
  0.6 187.6 %shard_map.143 = (bf16[768,2048]{1,0:T(8,128)(2,1)}, bf16[768,2048]{1,0:T(8,128)(2,1)}, f32[8,2048]{1,0:T(8,128)}, f32[2048,256]{1,0:T(8,128)}, f32[1,2048]{1,0:T(1,128)}) custom-call(bf16[768,2048]{1,0:T(8,128)(2,1)} %pg_ref.1, bf16[768,2048]{1,0:T(8,128)(2,1)} %pl_ref.1, f32[3,2048]{1,0:T(4,128)} %tg_ref.1, f32[3,2048]{1,0:T(4,128)} %tl_ref.1, ...), custom_call_target="tpu_custom_call" | custom-call | tf_op jit(solution)/shard_map/pallas_call | solution.py:321
  188.3 1.6 fusion.1
  189.8 1.5 fusion
  191.4 0.0 copy-start
  191.4 4.1 %copy.20 = bf16[768,2048]{1,0:T(8,128)(2,1)} copy(bf16[768,2048]{1,0:T(8,128)(2,1)} %get-tuple-element.30) | data formatting | bytes 6291456
  195.5 0.0 copy-done
  195.5 0.0 copy-start.1
  195.5 1.7 copy.21
  197.1 1.1 copy-done.1
  198.2 0.0 copy-start.2
  198.2 1.3 copy.22
  199.5 0.0 copy-done.2
  199.5 0.6 copy.23
Async XLA Ops:
  191.4 4.1 %copy-start = (bf16[768,2048]{1,0:T(8,128)(2,1)S(1)}, bf16[768,2048]{1,0:T(8,128)(2,1)}, u32[]{:S(2)}) copy-start(bf16[768,2048]{1,0:T(8,128)(2,1)} %get-tuple-element.31) | copy-start | bytes 9437188
  195.5 2.7 %copy-start.1 = (f32[2048,256]{1,0:T(8,128)S(1)}, f32[2048,256]{1,0:T(8,128)}, u32[]{:S(2)}) copy-start(f32[2048,256]{1,0:T(8,128)} %get-tuple-element.36) | copy-start | bytes 6291460
  198.2 1.3 copy-start.2
